TPU v7x, 32 devices: a whole 2x2x4 slice. The times are simulated.
32 devices in a mesh: sp: 8 (over z, x), tp: 4 (over y, core).
Axes of the slice: x: 2, y: 2, z: 4, core: 2. Of those that a mesh axis runs over, the one named last changes fastest.
Arguments:
- conv_value: bfloat16 [2048, 1024], P('sp', 'tp'), may hold values from -15 to 15
- conv_gate: bfloat16 [2048, 1024], P('sp', 'tp'), may hold values from -8 to 8
- conv_taps: bfloat16 [31, 1024], P(None, 'tp'), may hold values from -1 to 1
- conv_gain: float32 [1024], P('tp'), may hold values from 0.1 to 1.9
- out_weight: bfloat16 [1024, 2048], P('tp'), may hold values from -0.1875 to 0.1875
- residual: bfloat16 [2048, 2048], P('sp'), may hold values from -6 to 6
- route_ids: int32 [2048, 2], P('sp'), may hold values from 0 to 7, all different within a row; in each aligned block of 256 rows (0 to 255, 256 to 511, ...) at most 128 rows name the same one
- route_weight: float32 [2048, 2], P('sp'), may hold values from 0.3 to 1.5
- expert_gate: bfloat16 [8, 2048, 4096], P('sp', None, 'tp'), may hold values from -0.125 to 0.125
- expert_up: bfloat16 [8, 2048, 4096], P('sp', None, 'tp'), may hold values from -0.125 to 0.125
- expert_down: bfloat16 [8, 4096, 2048], P('sp', 'tp'), may hold values from -0.09375 to 0.09375
Outputs:
- layer_out: bfloat16 [2048, 2048], P('sp', 'tp')
Inputs may be any that keep to these rules, and one draw needn't show every extreme that they name: `route_ids`: in each aligned block of 256 rows no expert is named by more than 128 rows; some expert is named by exactly 128 rows in some blocks.
All inputs are finite; a program needn't handle non-finite values.
Results may differ from a plain program's by a relative error of at most 0.017.
Values may be sent and summed in bfloat16 or wider, within the bound.
A program may use at most 64 MiB of HBM per device.

v0:
```python
import jax
import jax.numpy as jnp
from jax import lax
from jax.sharding import PartitionSpec as P


def passed_along(value, axis, steps):
    count = lax.axis_size(axis)
    initial, last = (max(0, -steps), min(count, count - steps))
    return lax.ppermute(value, axis, [(source, source + steps) for source in range(initial, last)])


def slot_plan(block_ids, experts, capacity):
    assigned = block_ids.reshape(-1)
    pair_count = assigned.shape[0]
    onehot = (assigned[:, None] == jnp.arange(experts, dtype=jnp.int32)[None, :]).astype(jnp.int32)
    earlier = jnp.cumsum(onehot, axis=0) - onehot
    ranking = jnp.sum(earlier * onehot, axis=1)
    target = assigned * capacity + ranking
    owners = jnp.arange(pair_count, dtype=jnp.int32) // block_ids.shape[1]
    matches = target[None, :] == jnp.arange(experts * capacity, dtype=jnp.int32)[:, None]
    holder = jnp.sum(jnp.where(matches, owners[None, :] + 1, 0), axis=1) - 1
    holder = jnp.where(holder < 0, block_ids.shape[0], holder)
    return (target, holder)


def local(
    conv_value,
    conv_gate,
    conv_taps,
    conv_gain,
    out_weight,
    residual,
    route_ids,
    route_weight,
    expert_gate,
    expert_up,
    expert_down,
):
    taps_count = conv_taps.shape[0]
    token_rows = conv_value.shape[0]
    tails = passed_along(
        (conv_value[token_rows - taps_count + 1 :], conv_gate[token_rows - taps_count + 1 :]),
        "sp",
        1,
    )
    values_ext = jnp.concatenate([tails[0], conv_value], axis=0)
    gates_ext = jnp.concatenate([tails[1], conv_gate], axis=0)
    gated = values_ext.astype(jnp.float32) * jax.nn.sigmoid(gates_ext.astype(jnp.float32))
    filtered = jnp.zeros(conv_value.shape, jnp.float32)
    for offset in range(taps_count):
        filtered = (
            filtered + conv_taps[offset].astype(jnp.float32) * gated[offset : offset + token_rows]
        )
    channels = conv_value.shape[1] * lax.axis_size("tp")
    totals = lax.psum((jnp.sum(filtered, axis=1), jnp.sum(filtered * filtered, axis=1)), "tp")
    average = totals[0] / channels
    variance = totals[1] / channels - average * average
    normed = (filtered - average[:, None]) * lax.rsqrt(variance + 1e-05)[:, None] * conv_gain
    activated = jax.nn.silu(normed).astype(jnp.bfloat16)
    mixed = lax.psum(
        jnp.dot(activated, out_weight, preferred_element_type=jnp.float32).astype(jnp.bfloat16),
        "tp",
    ).astype(jnp.float32)
    updated = residual.astype(jnp.float32) + mixed
    width = updated.shape[1]
    normal_rows = (
        updated * lax.rsqrt(jnp.mean(updated * updated, axis=1, keepdims=True) + 1e-06)
    ).astype(jnp.bfloat16)
    experts = lax.axis_size("sp")
    top_count = route_ids.shape[1]
    capacity = 2 * token_rows * top_count // experts
    targets, holders = slot_plan(route_ids, experts, capacity)
    padded_rows = jnp.concatenate([normal_rows, jnp.zeros((1, width), jnp.bfloat16)], axis=0)
    buffer = padded_rows[holders].reshape(experts, capacity, width)
    w_gate = expert_gate[0]
    w_up = expert_up[0]
    w_down = expert_down[0]
    share = capacity // lax.axis_size("tp")
    mine = lax.dynamic_slice_in_dim(buffer, lax.axis_index("tp") * share, share, 1)
    arrived = lax.all_to_all(mine, "sp", split_axis=0, concat_axis=0, tiled=True)
    block = lax.all_gather(arrived, "tp", axis=1, tiled=True)
    flat = block.reshape(-1, width)
    gate_act = jnp.dot(flat, w_gate, preferred_element_type=jnp.float32)
    up_act = jnp.dot(flat, w_up, preferred_element_type=jnp.float32)
    hidden = (jax.nn.silu(gate_act) * up_act).astype(jnp.bfloat16)
    result = jnp.dot(hidden, w_down, preferred_element_type=jnp.float32)
    partials = result.reshape(block.shape[0], block.shape[1], width)
    summed = lax.psum_scatter(partials.astype(jnp.bfloat16), "tp", scatter_dimension=2, tiled=True)
    back = lax.all_to_all(summed, "sp", split_axis=0, concat_axis=0, tiled=True)
    columns = back.shape[2]
    picked = back.reshape(experts * capacity, columns)[targets].reshape(
        token_rows, top_count, columns
    )
    combined = jnp.sum(picked.astype(jnp.float32) * route_weight[:, :, None], axis=1)
    own_cols = lax.dynamic_slice_in_dim(updated, lax.axis_index("tp") * columns, columns, 1)
    return (own_cols + combined).astype(jnp.bfloat16)


def solution(mesh):
    placed = (
        P("sp", "tp"),
        P("sp", "tp"),
        P(None, "tp"),
        P("tp"),
        P("tp", None),
        P("sp", None),
        P("sp", None),
        P("sp", None),
        P("sp", None, "tp"),
        P("sp", None, "tp"),
        P("sp", "tp", None),
    )
    return jax.shard_map(
        local, mesh=mesh, in_specs=placed, out_specs=P("sp", "tp"), check_vma=False
    )
```

profile of v0, /device:TPU:0, one launch (start us, length us, event | category | flops | bytes accessed | tf_op | source)
XLA Modules:
  0.0 249.9 jit_solution(4921619316073596479)
XLA Ops:
  6.5 0.0 copy-start
  6.5 0.0 all-reduce.4.cloned.1.call-start
  6.5 0.8 slice.199
  7.4 4.9 %collective-permute-start = (bf16[30,256]{1,0:T(8,128)(2,1)S(1)}, bf16[30,256]{1,0:T(8,128)(2,1)S(1)}, u32[]{:S(2)}, u32[]{:S(2)}) collective-permute-start(bf16[30,256]{1,0:T(8,128)(2,1)S(1)} %slice.199), channel_id=1, source_target_pairs={{0,4},{4,8},{8,12},{12,16},{16,20},{20,24},{24,28},{1,5},{5,9},{9,... | collective-permute-start | bytes 46088 | tf_op jit(solution)/shard_map/ppermute | solution.py:10
  12.2 0.7 slice.200
  12.9 3.4 %collective-permute-start.1 = (bf16[30,256]{1,0:T(8,128)(2,1)S(1)}, bf16[30,256]{1,0:T(8,128)(2,1)S(1)}, u32[]{:S(2)}, u32[]{:S(2)}) collective-permute-start(bf16[30,256]{1,0:T(8,128)(2,1)S(1)} %slice.200), channel_id=1, source_target_pairs={{0,4},{4,8},{8,12},{12,16},{16,20},{20,24},{24,28},{1,5},{5,9},{9,... | collective-permute-start | bytes 46088 | tf_op jit(solution)/shard_map/ppermute | solution.py:10
  16.4 1.0 slice_convert_fusion.30
  17.4 1.0 slice_convert_fusion.29
  18.4 0.8 copy.17
  19.2 0.1 eq.39
  19.4 0.1 reshape.121
  19.5 1.1 reduce-window.6
  20.7 0.2 slice_reduce_fusion
  20.9 0.1 fusion.46
  21.0 0.3 select_reduce_fusion
  21.3 0.0 collective-permute-done
  21.3 0.0 collective-permute-done.1
  21.3 1.1 divide_multiply_fusion
  22.4 0.0 copy-start.8
  22.4 0.0 copy-start.1
  22.4 1.2 fusion.53
  23.6 6.0 %all-reduce.1 = (f32[256]{0:T(256)S(1)}, f32[256]{0:T(256)S(1)}) all-reduce(f32[256]{0:T(256)S(1)} %get-tuple-element.6, f32[256]{0:T(256)S(1)} %get-tuple-element.5), channel_id=1, replica_groups=mesh['sp'=8,'tp'=4] {'tp'}, use_global_device_ids=true, to_apply=%region_3.0 | all-reduce | flops 512 | bytes 4096 | tf_op jit(solution)/shard_map/psum | solution.py:56
  29.7 0.0 copy-done
  29.7 0.0 copy-done.8
  29.7 1.6 convolution_convert_fusion
  31.2 0.0 all-reduce.4.cloned.1.call-update
  31.2 0.0 all-gather.2.cloned.1.call-start
  31.3 36.4 %all-reduce.4.cloned.1.call-done = bf16[256,2048]{1,0:T(8,128)(2,1)} async-done(((bf16[256,2048]{1,0:T(8,128)(2,1)}), bf16[256,2048]{1,0:T(8,128)(2,1)}) %all-reduce.4.cloned.1.call-update) | async-done | bytes 1048592 | tf_op jit(solution)/shard_map/psum | solution.py:61
  67.8 0.0 copy-done.1
  67.8 0.0 copy-start.2
  67.8 3.0 %convert_add_fusion = (f32[256,2048]{1,0:T(8,128)}, f32[256]{0:T(256)S(1)}) fusion(bf16[256,2048]{1,0:T(8,128)(2,1)} %all-reduce.4.cloned.1.call-done, bf16[256,2048]{1,0:T(8,128)(2,1)S(1)} %copy-done.1), kind=kLoop, calls=%fused_computation.15 | loop fusion | flops 2621184 | bytes 4195328 | tf_op jit(solution)/shard_map/add | solution.py:65
  70.7 0.0 copy-done.2
  70.7 0.3 multiply_convert_fusion.1
  71.1 0.1 concatenate.11
  71.2 6.0 %gather_fusion = bf16[1024,2048]{1,0:T(8,128)(2,1)} fusion(bf16[257,2048]{1,0:T(8,128)(2,1)S(1)} %concatenate.11, s32[1024]{0:T(1024)S(1)} %broadcast_clamp_fusion), kind=kCustom, calls=%fused_computation | custom fusion | bytes 8392704 | tf_op jit(solution)/shard_map/gather | solution.py:75
  77.2 1.3 constant_dynamic-slice_fusion
  78.5 30.6 %all_to_all.10 = bf16[8,32,2048]{2,1,0:T(8,128)(2,1)} all-to-all(bf16[8,32,2048]{2,1,0:T(8,128)(2,1)S(1)} %constant_dynamic-slice_fusion), channel_id=1, replica_groups=mesh['sp'=8,'tp'=4] {'sp'}, dimensions={0} | all-to-all | bytes 2097152 | tf_op jit(solution)/shard_map/all_to_all | solution.py:81
  109.2 0.0 all-gather.2.cloned.1.call-update
  109.2 0.0 reduce-scatter.2.cloned.1.call-start
  109.2 33.4 %all-gather.2.cloned.1.call-done = bf16[8,128,2048]{2,1,0:T(8,128)(2,1)} async-done(((bf16[8,32,2048]{2,1,0:T(8,128)(2,1)}), bf16[8,128,2048]{2,1,0:T(8,128)(2,1)}) %all-gather.2.cloned.1.call-update) | async-done | bytes 4194320 | tf_op jit(solution)/shard_map/all_gather | solution.py:82
  142.7 0.0 copy-start.5
  142.7 0.0 copy-start.7
  142.7 7.7 %fusion.2 = f32[1024,1024]{1,0:T(8,128)S(1)} fusion(bf16[1024,2048]{1,0:T(8,128)(2,1)} %bitcast.102, bf16[1,2048,1024]{2,1,0:T(8,128)(2,1)} %param.20), kind=kOutput, calls=%fused_computation.4 | convolution fusion | flops 4294967296 | bytes 12582912 | tf_op jit(solution)/shard_map/dot_general | solution.py:85
  150.4 0.0 copy-done.5
  150.4 0.0 copy-done.7
  150.4 0.0 copy-start.6
  150.4 5.4 %multiply_convert_fusion = bf16[1024,1024]{1,0:T(8,128)(2,1)S(1)} fusion(f32[1024,1024]{1,0:T(8,128)S(1)} %fusion.2, bf16[1024,2048]{1,0:T(8,128)(2,1)S(1)} %bitcast.103, bf16[1,2048,1024]{2,1,0:T(8,128)(2,1)S(1)} %copy-done.5), kind=kOutput, calls=%fused_computation.8 | convolution fusion | flops 4301258752 | bytes 14680064 | tf_op jit(solution)/shard_map/dot_general | solution.py:84
  155.8 0.0 copy-done.6
  155.8 6.1 %fusion.6 = bf16[8,128,2048]{2,1,0:T(8,128)(2,1)} fusion(bf16[8,128,1024]{2,1,0:T(8,128)(2,1)S(1)} %bitcast.104, bf16[1,1024,2048]{2,1,0:T(8,128)(2,1)S(1)} %copy-done.6), kind=kOutput, calls=%fused_computation.9 | convolution fusion | flops 4297064448 | bytes 10485760 | tf_op jit(solution)/shard_map/dot_general | solution.py:87
  161.8 0.0 copy-start.3
  161.8 0.0 copy-start.4
  161.8 0.0 reduce-scatter.2.cloned.1.call-update
  161.9 44.5 %reduce-scatter.2.cloned.1.call-done = bf16[8,128,512]{2,1,0:T(8,128)(2,1)} async-done(((bf16[8,128,2048]{2,1,0:T(8,128)(2,1)}), bf16[8,128,512]{2,1,0:T(8,128)(2,1)}) %reduce-scatter.2.cloned.1.call-update) | async-done | bytes 1048592 | tf_op jit(solution)/shard_map/reduce_scatter | solution.py:89
  206.4 5.5 %all-to-all-start.1 = ((bf16[8,128,512]{2,1,0:T(8,128)(2,1)}), bf16[8,128,512]{2,1,0:T(8,128)(2,1)S(1)}, u32[]{:S(2)}, u32[]{:S(2)}) async-start(bf16[8,128,512]{2,1,0:T(8,128)(2,1)} %reduce-scatter.2.cloned.1.call-done), calls=%async_computation.2 | async-start | bytes 2097152 | tf_op jit(solution)/shard_map/all_to_all | solution.py:90
  211.9 0.0 copy-done.3
  211.9 0.1 copy.19
  212.1 0.1 mul.635
  212.2 0.0 copy-done.4
  212.2 0.1 copy.20
  212.4 25.2 %all-to-all-done.1 = bf16[8,128,512]{2,1,0:T(8,128)(2,1)S(1)} async-done(((bf16[8,128,512]{2,1,0:T(8,128)(2,1)}), bf16[8,128,512]{2,1,0:T(8,128)(2,1)S(1)}, u32[]{:S(2)}, u32[]{:S(2)}) %all-to-all-start.1) | async-done | bytes 1048608 | tf_op jit(solution)/shard_map/all_to_all | solution.py:90
  237.6 2.0 gather_fusion.1
  239.6 0.7 reshape.157
  240.2 1.3 multiply_reduce_fusion.1
  241.6 1.8 add_convert_fusion
  (12 shorter events, 0.1 us)
Async XLA Ops:
  6.5 23.1 %copy-start = (bf16[256,2048]{1,0:T(8,128)(2,1)S(1)}, bf16[256,2048]{1,0:T(8,128)(2,1)}, u32[]{:S(2)}) copy-start(bf16[256,2048]{1,0:T(8,128)(2,1)} %param.15) | copy-start | bytes 3145732
  6.5 61.2 %all-reduce.4.cloned.1.call-start = ((), (), s32[]{:S(2)}) async-start(), calls=%async_computation.3 | async-start | bytes 2097152 | tf_op jit(solution)/shard_map/psum | solution.py:61
  7.4 14.0 %collective-permute-start = (bf16[30,256]{1,0:T(8,128)(2,1)S(1)}, bf16[30,256]{1,0:T(8,128)(2,1)S(1)}, u32[]{:S(2)}, u32[]{:S(2)}) collective-permute-start(bf16[30,256]{1,0:T(8,128)(2,1)S(1)} %slice.199), channel_id=1, source_target_pairs={{0,4},{4,8},{8,12},{12,16},{16,20},{20,24},{24,28},{1,5},{5,9},{9,... | collective-permute-start | bytes 46088 | tf_op jit(solution)/shard_map/ppermute | solution.py:10
  12.9 8.4 %collective-permute-start.1 = (bf16[30,256]{1,0:T(8,128)(2,1)S(1)}, bf16[30,256]{1,0:T(8,128)(2,1)S(1)}, u32[]{:S(2)}, u32[]{:S(2)}) collective-permute-start(bf16[30,256]{1,0:T(8,128)(2,1)S(1)} %slice.200), channel_id=1, source_target_pairs={{0,4},{4,8},{8,12},{12,16},{16,20},{20,24},{24,28},{1,5},{5,9},{9,... | collective-permute-start | bytes 46088 | tf_op jit(solution)/shard_map/ppermute | solution.py:10
  22.4 7.2 %copy-start.8 = (f32[256]{0:T(256)S(1)}, f32[256]{0:T(256)}, u32[]{:S(2)}) copy-start(f32[256]{0:T(256)} %param.14) | copy-start | bytes 3076
  22.4 45.3 %copy-start.1 = (bf16[256,2048]{1,0:T(8,128)(2,1)S(1)}, bf16[256,2048]{1,0:T(8,128)(2,1)}, u32[]{:S(2)}) copy-start(bf16[256,2048]{1,0:T(8,128)(2,1)} %param.16) | copy-start | bytes 3145732
  31.2 111.5 %all-gather.2.cloned.1.call-start = ((), (), s32[]{:S(2)}) async-start(), calls=%async_computation.4 | async-start | bytes 5242880 | tf_op jit(solution)/shard_map/all_gather | solution.py:82
  67.8 3.0 %copy-start.2 = (bf16[256,2048]{1,0:T(8,128)(2,1)S(1)}, bf16[256,2048]{1,0:T(8,128)(2,1)}, u32[]{:S(2)}) copy-start(bf16[256,2048]{1,0:T(8,128)(2,1)} %all-reduce.4.cloned.1.call-done) | copy-start | bytes 3145732
  109.2 97.2 %reduce-scatter.2.cloned.1.call-start = ((), (), s32[]{:S(2)}) async-start(), calls=%async_computation.5 | async-start | bytes 5242880 | tf_op jit(solution)/shard_map/reduce_scatter | solution.py:89
  142.7 7.7 %copy-start.5 = (bf16[1,2048,1024]{2,1,0:T(8,128)(2,1)S(1)}, bf16[1,2048,1024]{2,1,0:T(8,128)(2,1)}, u32[]{:S(2)}) copy-start(bf16[1,2048,1024]{2,1,0:T(8,128)(2,1)} %param.19) | copy-start | bytes 12582916
  142.7 7.7 %copy-start.7 = (bf16[8,128,2048]{2,1,0:T(8,128)(2,1)S(1)}, bf16[8,128,2048]{2,1,0:T(8,128)(2,1)}, u32[]{:S(2)}) copy-start(bf16[8,128,2048]{2,1,0:T(8,128)(2,1)} %all-gather.2.cloned.1.call-done) | copy-start | bytes 12582916
  150.4 5.4 %copy-start.6 = (bf16[1,1024,2048]{2,1,0:T(8,128)(2,1)S(1)}, bf16[1,1024,2048]{2,1,0:T(8,128)(2,1)}, u32[]{:S(2)}) copy-start(bf16[1,1024,2048]{2,1,0:T(8,128)(2,1)} %param.21) | copy-start | bytes 12582916
  161.8 50.1 %copy-start.3 = (s32[256,2]{0,1:T(2,128)S(1)}, s32[256,2]{0,1:T(2,128)}, u32[]{:S(2)}) copy-start(s32[256,2]{0,1:T(2,128)} %param.17) | copy-start | bytes 6148
  161.8 50.4 %copy-start.4 = (f32[256,2]{0,1:T(2,128)S(1)}, f32[256,2]{0,1:T(2,128)}, u32[]{:S(2)}) copy-start(f32[256,2]{0,1:T(2,128)} %param.18) | copy-start | bytes 6148
  206.4 31.2 %all-to-all-start.1 = ((bf16[8,128,512]{2,1,0:T(8,128)(2,1)}), bf16[8,128,512]{2,1,0:T(8,128)(2,1)S(1)}, u32[]{:S(2)}, u32[]{:S(2)}) async-start(bf16[8,128,512]{2,1,0:T(8,128)(2,1)} %reduce-scatter.2.cloned.1.call-done), calls=%async_computation.2 | async-start | bytes 2097152 | tf_op jit(solution)/shard_map/all_to_all | solution.py:90
Sparse Core Ops, SparseCore 0:
  31.4 36.3 all-reduce.3
  109.3 33.3 all-gather.1
  162.0 44.3 reduce-scatter.1
where the time goes:
time: 250 us
  waiting for transfers between devices  140 us (56%)
  blocking collectives  36.7 us (15%)
  matrix products  20.6 us (8%)
  starting transfers between devices  13.9 us (6%)
  local copies, waits for them, and re-layouts  13.4 us (5%)
  between operations  13.4 us (5%)
  other arithmetic  12.3 us (5%)
    reduce_scatter x1, waiting for transfers between devices, local(): lax.psum_scatter(partials.astype(jnp.bfloat16), 'tp', scatter_dimension=2...  44.5 us
    psum x1, waiting for transfers between devices, local(): lax.psum(jnp.dot(activated, out_weight, preferred_element_type=jnp.float3...  36.4 us
    all_gather x1, waiting for transfers between devices, local(): block = lax.all_gather(arrived, 'tp', axis=1, tiled=True)  33.4 us
    all_to_all x1, blocking collectives, local(): lax.all_to_all(mine, 'sp', split_axis=0, concat_axis=0, tiled=True)  30.6 us
    all_to_all x1, waiting for transfers between devices, local(): back = lax.all_to_all(summed, 'sp', split_axis=0, concat_axis=0, tiled=True)  25.2 us
    ppermute x2, starting transfers between devices, passed_along(): lax.ppermute(value, axis, [(source, source + steps) for source in range(i...  8.3 us
    dot_general x1, matrix products, local(): up_act = jnp.dot(flat, w_up, preferred_element_type=jnp.float32)  7.65 us
    dot_general x1, matrix products, local(): result = jnp.dot(hidden, w_down, preferred_element_type=jnp.float32)  6.07 us
  transfers between devices with their start and end apart: 6, of which 4 were waited for; matrix products, arithmetic and copies ran while one was open for 2% of the time, Pallas kernels for 0%

commit v1 on v0

v1 whole, which is shorter than its diff:
```python
import functools

import jax
import jax.numpy as jnp
from jax import lax
from jax.experimental import pallas as pl
from jax.experimental.pallas import tpu as pltpu
from jax.sharding import PartitionSpec as P

MESH = pl.DeviceIdType.MESH
F32 = jnp.float32
BF16 = jnp.bfloat16


def passed_along(value, axis, steps):
    count = lax.axis_size(axis)
    initial, last = (max(0, -steps), min(count, count - steps))
    return lax.ppermute(value, axis, [(source, source + steps) for source in range(initial, last)])


def partner(me, d, n):
    if n & (n - 1):
        raise ValueError("sp size")
    out, w = me, 1
    while w < n:
        if d & w:
            out = out + w * (1 - 2 * lax.rem(lax.div(me, w), 2))
        w *= 2
    return out


def ffn_kernel(
    n_sp, n_tp, cap, order, group,
    send, tgt, rw, own, wg_hbm, wu_hbm, wd_hbm, out,
    wg, wu, wd, X, xs, hid, pown, pcs, pcr, q, pys, pyr, eo, back,
    w_sem, l_sem, a_s, a_r, c_s, c_r, y_s, y_r, f_s, f_r, pc_s, pc_r, py_s, py_r, b_s, b_r,
):
    Y = n_tp // 2
    S = n_sp // group
    C = send.shape[1]
    R = cap * group
    me = lax.axis_index("sp")
    t = lax.axis_index("tp")
    y = lax.div(t, 2)
    c = lax.rem(t, 2)
    core = t + 1 - 2 * c

    def ypeer(k):
        return lax.rem(y + k, Y) * 2 + c

    loads = [
        pltpu.make_async_copy(src, dst, w_sem.at[i])
        for i, (src, dst) in enumerate(((wg_hbm, wg), (wu_hbm, wu), (wd_hbm, wd)))
    ]
    for cp in loads:
        cp.start()

    barrier = pltpu.get_barrier_semaphore()
    for d in range(1, n_sp):
        pl.semaphore_signal(barrier, inc=1, device_id=(partner(me, d, n_sp), t), device_id_type=MESH)
    pl.semaphore_signal(barrier, inc=1, device_id=(me, core), device_id_type=MESH)
    for k in range(1, Y):
        pl.semaphore_signal(barrier, inc=1, device_id=(me, ypeer(k)), device_id_type=MESH)
    pl.semaphore_wait(barrier, n_sp - 1 + 1 + Y - 1)

    def remote(src, dst, s_sem, r_sem, dev):
        cp = pltpu.make_async_remote_copy(
            src_ref=src, dst_ref=dst, send_sem=s_sem, recv_sem=r_sem, device_id=dev, device_id_type=MESH
        )
        cp.start()
        return cp

    sent = []
    arrive = {}
    for p, d in enumerate(order):
        dst = partner(me, d, n_sp)
        src = send.at[pl.ds(pl.multiple_of(dst * cap, cap), cap)]
        to = X.at[t, pl.ds(p * cap, cap)]
        if d == 0:
            cp = pltpu.make_async_copy(src, to, l_sem.at[0])
            cp.start()
            arrive[p] = cp
        else:
            cp = remote(src, to, a_s.at[p], a_r.at[p], (dst, t))
            sent.append(cp)
            arrive[p] = cp

    ag_c, ag_y, ag_f, rs_c, rs_y, ret = {}, {}, {}, {}, {}, {}

    def rows(s):
        return pl.ds(s * R, R)

    def stage_a(s):
        for p in range(s * group, (s + 1) * group):
            if order[p] == 0:
                arrive[p].wait()
            else:
                arrive[p].wait_recv()
        mine = X.at[t, rows(s)]
        for k in range(1, Y):
            i = s * Y + k
            ag_y[s, k] = remote(mine, mine, y_s.at[i], y_r.at[i], (me, ypeer(k)))
        ag_c[s] = remote(mine, mine, c_s.at[s], c_r.at[s], (me, core))

    def stage_b(s):
        for k in range(1, Y):
            ag_y[s, k].wait_recv()
            i = s * Y + k
            got = X.at[lax.rem(y + Y - k, Y) * 2 + c, rows(s)]
            ag_f[s, k] = remote(got, got, f_s.at[i], f_r.at[i], (me, core))

    tile = 256

    def stage_c(s):
        ag_c[s].wait_recv()
        for k in range(1, Y):
            ag_f[s, k].wait_recv()
        for j in range(n_tp):
            xs[:, j * C:(j + 1) * C] = X[j, rows(s), :]
        if s == 0:
            for cp in loads:
                cp.wait()

        def up(n, carry):
            cols = pl.ds(pl.multiple_of(n * tile, tile), tile)
            x = xs[...]
            g = jnp.dot(x, wg[:, cols], preferred_element_type=F32)
            u = jnp.dot(x, wu[:, cols], preferred_element_type=F32)
            hid[:, cols] = (g / (1.0 + jnp.exp(-g)) * u).astype(BF16)
            return carry

        lax.fori_loop(0, hid.shape[1] // tile, up, 0)

        def theirs(yy, carry):
            cols = pl.ds(pl.multiple_of((yy * 2 + 1 - c) * C, C), C)
            pcs[s, yy] = jnp.dot(hid[...], wd[:, cols], preferred_element_type=F32).astype(BF16)
            return carry

        lax.fori_loop(0, Y, theirs, 0)
        rs_c[s] = remote(pcs.at[s], pcr.at[s], pc_s.at[s], pc_r.at[s], (me, core))

        def ours(yy, carry):
            cols = pl.ds(pl.multiple_of((yy * 2 + c) * C, C), C)
            pown[yy] = jnp.dot(hid[...], wd[:, cols], preferred_element_type=F32)
            return carry

        lax.fori_loop(0, Y, ours, 0)

    def stage_d(s):
        rs_c[s].wait_recv()
        for k in range(1, Y):
            yy = lax.rem(y + k, Y)
            i = s * Y + k
            pys[i] = (pown[yy] + pcr[s, yy].astype(F32)).astype(BF16)
            rs_y[s, k] = remote(pys.at[i], pyr.at[i], py_s.at[i], py_r.at[i], (me, ypeer(k)))
        q[s] = pown[y] + pcr[s, y].astype(F32)

    def stage_e(s):
        total = q[s]
        for k in range(1, Y):
            rs_y[s, k].wait_recv()
            total = total + pyr[s * Y + k].astype(F32)
        eo[rows(s)] = total.astype(BF16)
        for p in range(s * group, (s + 1) * group):
            d = order[p]
            dst = partner(me, d, n_sp)
            src = eo.at[pl.ds(p * cap, cap)]
            to = back.at[pl.ds(pl.multiple_of(me * cap, cap), cap)]
            if d == 0:
                cp = pltpu.make_async_copy(src, to, l_sem.at[1])
                cp.start()
            else:
                cp = remote(src, to, b_s.at[p], b_r.at[p], (dst, t))
            ret[p] = cp

    stage_a(0)
    stage_b(0)
    for s in range(S):
        if s + 1 < S:
            stage_a(s + 1)
        stage_c(s)
        if s + 1 < S:
            stage_b(s + 1)
        stage_d(s)
        if s > 0:
            stage_e(s - 1)
    stage_e(S - 1)

    for p, d in enumerate(order):
        if d == 0:
            ret[p].wait()
        else:
            ret[p].wait_recv()
    total = own[...]
    places = lax.broadcasted_iota(jnp.int32, (total.shape[0], back.shape[0]), 1)
    for k in range(tgt.shape[1]):
        pick = jnp.where(places == tgt[:, k:k + 1], 1.0, 0.0).astype(BF16)
        total = total + rw[:, k:k + 1] * jnp.dot(pick, back[...], preferred_element_type=F32)
    out[...] = total.astype(BF16)

    for cp in sent:
        cp.wait_send()
    for table in (ag_c, ag_y, ag_f, rs_c, rs_y):
        for cp in table.values():
            cp.wait_send()
    for p, d in enumerate(order):
        if d != 0:
            ret[p].wait_send()


def routed_ffn(send, targets, route_weight, own, w_gate, w_up, w_down, cap):
    n_sp, n_tp = lax.axis_size("sp"), lax.axis_size("tp")
    group = max(1, min(n_sp, 256 // cap))
    order = list(range(n_sp))
    if n_sp == 8:
        order = [0, 1, 4, 5, 6, 7, 2, 3]
    S, Y, C, R = n_sp // group, n_tp // 2, send.shape[1], cap * group
    width, hidden = w_gate.shape
    tokens = own.shape[0]
    dma = pltpu.SemaphoreType.DMA
    vm = pl.BlockSpec(memory_space=pltpu.VMEM)
    hb = pl.BlockSpec(memory_space=pl.ANY)
    return pl.pallas_call(
        functools.partial(ffn_kernel, n_sp, n_tp, cap, order, group),
        out_shape=jax.ShapeDtypeStruct((tokens, C), BF16),
        in_specs=[vm, vm, vm, vm, hb, hb, hb],
        out_specs=vm,
        scratch_shapes=[
            pltpu.VMEM((width, hidden), BF16),
            pltpu.VMEM((width, hidden), BF16),
            pltpu.VMEM((hidden, width), BF16),
            pltpu.VMEM((n_tp, n_sp * cap, C), BF16),
            pltpu.VMEM((R, width), BF16),
            pltpu.VMEM((R, hidden), BF16),
            pltpu.VMEM((Y, R, C), F32),
            pltpu.VMEM((S, Y, R, C), BF16),
            pltpu.VMEM((S, Y, R, C), BF16),
            pltpu.VMEM((S, R, C), F32),
            pltpu.VMEM((S * Y, R, C), BF16),
            pltpu.VMEM((S * Y, R, C), BF16),
            pltpu.VMEM((n_sp * cap, C), BF16),
            pltpu.VMEM((n_sp * cap, C), BF16),
            dma((3,)), dma((2,)),
            dma((n_sp,)), dma((n_sp,)),
            dma((S,)), dma((S,)),
            dma((S * Y,)), dma((S * Y,)),
            dma((S * Y,)), dma((S * Y,)),
            dma((S,)), dma((S,)),
            dma((S * Y,)), dma((S * Y,)),
            dma((n_sp,)), dma((n_sp,)),
        ],
        compiler_params=pltpu.CompilerParams(
            collective_id=1, has_side_effects=True, vmem_limit_bytes=60 * 1024 * 1024
        ),
    )(send, targets, route_weight, own, w_gate, w_up, w_down)


def slot_targets(block_ids, experts, capacity):
    assigned = block_ids.reshape(-1)
    onehot = (assigned[:, None] == jnp.arange(experts, dtype=jnp.int32)[None, :]).astype(jnp.int32)
    earlier = jnp.cumsum(onehot, axis=0) - onehot
    ranking = jnp.sum(earlier * onehot, axis=1)
    return (assigned * capacity + ranking).reshape(block_ids.shape)


def local(
    conv_value,
    conv_gate,
    conv_taps,
    conv_gain,
    out_weight,
    residual,
    route_ids,
    route_weight,
    expert_gate,
    expert_up,
    expert_down,
):
    taps_count = conv_taps.shape[0]
    token_rows = conv_value.shape[0]
    experts = lax.axis_size("sp")
    top_count = route_ids.shape[1]
    capacity = 2 * token_rows * top_count // experts
    targets = slot_targets(route_ids, experts, capacity)
    tails = passed_along(
        jnp.concatenate(
            [conv_value[token_rows - taps_count + 1:], conv_gate[token_rows - taps_count + 1:]], axis=1
        ),
        "sp",
        1,
    )
    chans = conv_value.shape[1]
    values_ext = jnp.concatenate([tails[:, :chans], conv_value], axis=0)
    gates_ext = jnp.concatenate([tails[:, chans:], conv_gate], axis=0)
    gated = values_ext.astype(F32) * jax.nn.sigmoid(gates_ext.astype(F32))
    filtered = jnp.zeros(conv_value.shape, F32)
    for offset in range(taps_count):
        filtered = filtered + conv_taps[offset].astype(F32) * gated[offset:offset + token_rows]
    channels = chans * lax.axis_size("tp")
    totals = lax.psum((jnp.sum(filtered, axis=1), jnp.sum(filtered * filtered, axis=1)), "tp")
    average = totals[0] / channels
    variance = totals[1] / channels - average * average
    normed = (filtered - average[:, None]) * lax.rsqrt(variance + 1e-05)[:, None] * conv_gain
    activated = jax.nn.silu(normed).astype(BF16)
    mixed = lax.psum_scatter(
        jnp.dot(activated, out_weight, preferred_element_type=F32).astype(BF16),
        "tp", scatter_dimension=1, tiled=True,
    ).astype(F32)
    width = residual.shape[1]
    columns = mixed.shape[1]
    own = lax.dynamic_slice_in_dim(residual, lax.axis_index("tp") * columns, columns, 1).astype(F32) + mixed
    squares = lax.psum(jnp.sum(own * own, axis=1, keepdims=True), "tp") / width
    normal = (own * lax.rsqrt(squares + 1e-06)).astype(BF16)
    slots = jnp.arange(experts * capacity, dtype=jnp.int32)
    pick = functools.reduce(
        jnp.logical_or, [slots[:, None] == targets[None, :, k] for k in range(top_count)]
    ).astype(BF16)
    send = jnp.dot(pick, normal, preferred_element_type=F32).astype(BF16)
    return routed_ffn(
        send, targets, route_weight, own, expert_gate[0], expert_up[0], expert_down[0], capacity
    )


def solution(mesh):
    placed = (
        P("sp", "tp"),
        P("sp", "tp"),
        P(None, "tp"),
        P("tp"),
        P("tp", None),
        P("sp", None),
        P("sp", None),
        P("sp", None),
        P("sp", None, "tp"),
        P("sp", None, "tp"),
        P("sp", "tp", None),
    )
    return jax.shard_map(
        local, mesh=mesh, in_specs=placed, out_specs=P("sp", "tp"), check_vma=False
    )
```

time: 250 us -> 147 us (0.59)
  waiting for transfers between devices: 140 us -> 22.9 us
  Pallas kernels: 0 us -> 78.4 us
  blocking collectives: 36.7 us -> 12.1 us
  matrix products: 20.6 us -> 3.03 us
  starting transfers between devices: 13.9 us -> 4.87 us
  local copies, waits for them, and re-layouts: 13.4 us -> 5.14 us
  other arithmetic: 12.3 us -> 6.73 us
    pallas_call x0 -> x1, Pallas kernels: none -> 78.4 us  [routed_ffn(): pl.pallas_call(functools.partial(ffn_kernel, n_sp, n_tp, cap, order, grou...]
    psum x1 -> x0, waiting for transfers between devices: 36.4 us -> none  [local(): lax.psum(jnp.dot(activated, out_weight, preferred_element_type=jnp.float3...]
    all_gather x1 -> x0, waiting for transfers between devices: 33.4 us -> none  [local(): block = lax.all_gather(arrived, 'tp', axis=1, tiled=True)]
    all_to_all x1 -> x0, blocking collectives: 30.6 us -> none  [local(): lax.all_to_all(mine, 'sp', split_axis=0, concat_axis=0, tiled=True)]
    all_to_all x1 -> x0, waiting for transfers between devices: 25.2 us -> none  [local(): back = lax.all_to_all(summed, 'sp', split_axis=0, concat_axis=0, tiled=True)]
    reduce_scatter x1, waiting for transfers between devices: 44.5 us -> 22.9 us  [local(): lax.psum_scatter(jnp.dot(activated, out_weight, preferred_element_type=F3...]
    dot_general x4 -> x2, matrix products: 20.6 us -> 3.03 us  [the longest x1 1.52 us: local(): send = jnp.dot(pick, normal, preferred_element_type=F32).astype(BF16)]
    gather x2 -> x0, local copies, waits for them, and re-layouts: 7.98 us -> none  [the longest x1 6.02 us: local(): buffer = padded_rows[holders].reshape(experts, capacity, width)]
  transfers between devices with their start and end apart: 6 -> 2, of which waited for: 4 -> 1; matrix products, arithmetic and copies ran while one was open for 2% -> 4% of each run, Pallas kernels for 0% -> 0%
where the time goes in v1:
time: 147 us
  Pallas kernels  78.4 us (53%)
  waiting for transfers between devices  22.9 us (16%)
  between operations  13.6 us (9%)
  blocking collectives  12.1 us (8%)
  other arithmetic  6.73 us (5%)
  local copies, waits for them, and re-layouts  5.14 us (3%)
  starting transfers between devices  4.87 us (3%)
  matrix products  3.03 us (2%)
    pallas_call x1, Pallas kernels, routed_ffn(): pl.pallas_call(functools.partial(ffn_kernel, n_sp, n_tp, cap, order, grou...  78.4 us
    reduce_scatter x1, waiting for transfers between devices, local(): lax.psum_scatter(jnp.dot(activated, out_weight, preferred_element_type=F3...  22.9 us
    psum x1, blocking collectives, local(): lax.psum((jnp.sum(filtered, axis=1), jnp.sum(filtered * filtered, axis=1)...  6.33 us
    psum x1, blocking collectives, local(): squares = lax.psum(jnp.sum(own * own, axis=1, keepdims=True), 'tp') / width  5.76 us
    ppermute x1, starting transfers between devices, passed_along(): lax.ppermute(value, axis, [(source, source + steps) for source in range(i...  4.87 us
  transfers between devices with their start and end apart: 2, of which 1 were waited for; matrix products, arithmetic and copies ran while one was open for 4% of the time, Pallas kernels for 0%

profile of v1, /device:TPU:0, one launch (start us, length us, event | category | flops | bytes accessed | tf_op | source)
XLA Modules:
  0.0 146.7 jit_solution(16526970259767547917)
XLA Ops:
  6.5 0.0 copy-start
  6.5 0.0 reduce-scatter.2.cloned.1.call-start
  6.5 0.8 slice.215
  7.4 0.7 slice.216
  8.1 4.9 %collective-permute-start = (bf16[30,512]{1,0:T(8,128)(2,1)S(1)}, bf16[30,512]{1,0:T(8,128)(2,1)S(1)}, u32[]{:S(2)}, u32[]{:S(2)}) collective-permute-start(bf16[30,512]{1,0:T(8,128)(2,1)S(1)} %pad_maximum_fusion), channel_id=1, source_target_pairs={{0,4},{4,8},{8,12},{12,16},{16,20},{20,24},{24,28},{1,5},{5,9},{9,... | collective-permute-start | bytes 92168 | tf_op jit(solution)/shard_map/ppermute | solution.py:18
  13.0 1.0 slice_convert_fusion.30
  14.0 1.0 slice_convert_fusion.29
  15.0 0.0 collective-permute-done
  15.0 1.1 divide_multiply_fusion
  16.1 0.0 copy-start.5
  16.1 0.0 copy-start.3
  16.1 1.1 fusion.43
  17.2 0.0 copy-start.4
  17.2 6.3 %all-reduce = (f32[256]{0:T(256)S(1)}, f32[256]{0:T(256)S(1)}) all-reduce(f32[256]{0:T(256)S(1)} %get-tuple-element.6, f32[256]{0:T(256)S(1)} %get-tuple-element.5), channel_id=1, replica_groups=mesh['sp'=8,'tp'=4] {'tp'}, use_global_device_ids=true, to_apply=%region_6.7 | all-reduce | flops 512 | bytes 4096 | tf_op jit(solution)/shard_map/psum | solution.py:300
  23.6 0.0 copy-done
  23.6 0.0 copy-done.5
  23.6 1.5 %convolution_convert_fusion = bf16[256,2048]{1,0:T(8,128)(2,1)} fusion(bf16[256,2048]{1,0:T(8,128)(2,1)S(1)} %copy-done, f32[256,256]{1,0:T(8,128)S(1)} %get-tuple-element.13, f32[256]{0:T(256)S(1)} %copy-done.5, f32[256]{0:T(256)S(1)} %get-tuple-element.48, f32[256]{0:T(256)S(1)} %get-tuple-element.47), kind=kOutput, calls=%fused_computation | convolution fusion | flops 269484032 | bytes 2362368 | tf_op jit(solution)/shard_map/dot_general | solution.py:306
  25.1 0.0 reduce-scatter.2.cloned.1.call-update
  25.1 0.0 copy-done.3
  25.1 0.1 copy.20
  25.3 0.1 eq.60
  25.4 0.1 eq.56
  25.6 0.1 copy.22
  25.7 1.1 reduce-window.6
  26.9 0.2 slice_reduce_fusion.2
  27.1 0.1 fusion.40
  27.2 0.1 reduce_sum.39
  27.4 0.0 copy-done.4
  27.4 0.8 copy.23.rw
  28.2 0.0 copy-start.1
  28.2 0.2 slice_reduce_fusion.1
  28.4 22.9 %reduce-scatter.2.cloned.1.call-done = bf16[256,512]{1,0:T(8,128)(2,1)} async-done(((bf16[256,2048]{1,0:T(8,128)(2,1)}), bf16[256,512]{1,0:T(8,128)(2,1)}) %reduce-scatter.2.cloned.1.call-update) | async-done | bytes 262160 | tf_op jit(solution)/shard_map/reduce_scatter | solution.py:305
  51.3 1.2 multiply_reduce_fusion
  52.5 0.0 copy-start.2
  52.5 5.8 %psum.23 = f32[256,1]{0,1:T(1,128)S(1)} all-reduce(f32[256,1]{0,1:T(1,128)S(1)} %bitcast.79), channel_id=1, replica_groups=mesh['sp'=8,'tp'=4] {'tp'}, use_global_device_ids=true, to_apply=%region_9.10 | all-reduce | flops 256 | bytes 2048 | tf_op jit(solution)/shard_map/psum | solution.py:312
  58.2 1.5 %convolution_convert_fusion.1.send = bf16[1024,512]{1,0:T(8,128)(2,1)} fusion(s32[256]{0:T(256)S(1)} %get-tuple-element.8, s32[256]{0:T(256)S(1)} %get-tuple-element.7, f32[256,512]{1,0:T(8,128)S(1)} %get-tuple-element.12.own, f32[256]{0:T(256)S(1)} %bitcast.80), kind=kOutput, calls=%fused_computation.1 | convolution fusion | flops 270008320 | bytes 1575936 | tf_op jit(solution)/shard_map/dot_general | solution.py:318
  59.8 0.0 copy-done.1
  59.8 0.0 copy-done.2
  59.8 78.4 %shard_map.109 = bf16[256,512]{1,0:T(8,128)(2,1)} custom-call(bf16[1024,512]{1,0:T(8,128)(2,1)} %convolution_convert_fusion.1.send, s32[256,2]{1,0:T(8,128)} %copy-done.1, f32[256,2]{1,0:T(8,128)} %copy.23.rw, f32[256,512]{1,0:T(8,128)} %copy-done.2, bf16[2048,1024]{1,0:T(8,128)(2,1)} %bitcast.45, bf16[2048,1024]{1,0:T(8,128)(2,1)} %bitcast.46, ...), custom_call_target="tpu_custom_call" | custom-call | tf_op jit(solution)/shard_map/pallas_call | solution.py:223
  138.2 1.7 %copy.25 = bf16[256,512]{1,0:T(8,128)(2,1)} copy(bf16[256,512]{1,0:T(8,128)(2,1)} %shard_map.109) | data formatting | bytes 524288
  (9 shorter events, 0.1 us)
Async XLA Ops:
  6.5 17.0 %copy-start = (bf16[256,2048]{1,0:T(8,128)(2,1)S(1)}, bf16[256,2048]{1,0:T(8,128)(2,1)}, u32[]{:S(2)}) copy-start(bf16[256,2048]{1,0:T(8,128)(2,1)} %param.15) | copy-start | bytes 3145732
  6.5 44.7 %reduce-scatter.2.cloned.1.call-start = ((), (), s32[]{:S(2)}) async-start(), calls=%async_computation.1 | async-start | bytes 1310720 | tf_op jit(solution)/shard_map/reduce_scatter | solution.py:305
  8.1 6.9 %collective-permute-start = (bf16[30,512]{1,0:T(8,128)(2,1)S(1)}, bf16[30,512]{1,0:T(8,128)(2,1)S(1)}, u32[]{:S(2)}, u32[]{:S(2)}) collective-permute-start(bf16[30,512]{1,0:T(8,128)(2,1)S(1)} %pad_maximum_fusion), channel_id=1, source_target_pairs={{0,4},{4,8},{8,12},{12,16},{16,20},{20,24},{24,28},{1,5},{5,9},{9,... | collective-permute-start | bytes 92168 | tf_op jit(solution)/shard_map/ppermute | solution.py:18
  16.1 7.5 %copy-start.5 = (f32[256]{0:T(256)S(1)}, f32[256]{0:T(256)}, u32[]{:S(2)}) copy-start(f32[256]{0:T(256)} %param.14) | copy-start | bytes 3076
  16.1 9.1 %copy-start.3 = (s32[256,2]{0,1:T(2,128)S(1)}, s32[256,2]{0,1:T(2,128)}, u32[]{:S(2)}) copy-start(s32[256,2]{0,1:T(2,128)} %param.17) | copy-start | bytes 6148
  17.2 10.2 %copy-start.4 = (f32[256,2]{0,1:T(2,128)S(1)}, f32[256,2]{0,1:T(2,128)}, u32[]{:S(2)}) copy-start(f32[256,2]{0,1:T(2,128)} %param.18) | copy-start | bytes 6148
  28.2 31.6 %copy-start.1 = (s32[256,2]{1,0:T(8,128)}, s32[256,2]{1,0:T(8,128)S(1)}, u32[]{:S(2)}) copy-start(s32[256,2]{1,0:T(8,128)S(1)} %add.127.tgt) | copy-start | bytes 6148
  52.5 7.3 %copy-start.2 = (f32[256,512]{1,0:T(8,128)}, f32[256,512]{1,0:T(8,128)S(1)}, u32[]{:S(2)}) copy-start(f32[256,512]{1,0:T(8,128)S(1)} %get-tuple-element.12.own) | copy-start | bytes 1572868
Sparse Core Ops, SparseCore 0:
  25.2 25.9 reduce-scatter.1

commit v2 on v1

v2 whole, which is shorter than its diff:
```python
import functools

import jax
import jax.numpy as jnp
from jax import lax
from jax.experimental import pallas as pl
from jax.experimental.pallas import tpu as pltpu
from jax.sharding import PartitionSpec as P

MESH = pl.DeviceIdType.MESH
F32 = jnp.float32
BF16 = jnp.bfloat16


def partner(me, d, n):
    if n & (n - 1):
        raise ValueError("sp size")
    out, w = me, 1
    while w < n:
        if d & w:
            out = out + w * (1 - 2 * lax.rem(lax.div(me, w), 2))
        w *= 2
    return out


def as_row(first, second):
    lanes = lax.broadcasted_iota(jnp.int32, (first.shape[0], 128), 1)
    both = jnp.where(lanes == 0, first, jnp.where(lanes == 1, second, 0.0))
    return both.T[0:8]


def as_columns(rows8):
    return jnp.concatenate([rows8] * 16, axis=0).T


def stacked(rows):
    place = lax.broadcasted_iota(jnp.int32, (8, rows[0].shape[1]), 0)
    out = jnp.zeros((8, rows[0].shape[1]), F32)
    for i, r in enumerate(rows):
        out = jnp.where(place == i, r, out)
    return out


def layer_kernel(
    n_sp, n_tp, cap, order, group, halo_rows,
    value, gate, taps, gain, ids, rwt, ow_hbm, res_hbm, wg_hbm, wu_hbm, wd_hbm, out,
    ow, res, halo, G, fil, st_s, st_r, act, p1s, p1r, p1own, y1s, y1r, own, nrm, pickt, meta, send,
    wg, wu, wd, X, xs, hid, pown, pcs, pcr, q, pys, pyr, eo, back,
    o_sem, h_s, h_r, s_s, s_r, p1_s, p1_r, y1_s, y1_r,
    w_sem, l_sem, a_s, a_r, c_s, c_r, y_s, y_r, f_s, f_r, pc_s, pc_r, py_s, py_r, b_s, b_r,
):
    Y = n_tp // 2
    S = n_sp // group
    C = send.shape[1]
    R = cap * group
    T, chans = value.shape
    taps_count = taps.shape[0]
    top = ids.shape[0]
    me = lax.axis_index("sp")
    t = lax.axis_index("tp")
    y = lax.div(t, 2)
    c = lax.rem(t, 2)
    core = t + 1 - 2 * c

    def ypeer(k):
        return lax.rem(y + k, Y) * 2 + c

    barrier = pltpu.get_barrier_semaphore()
    for d in range(1, n_sp):
        pl.semaphore_signal(barrier, inc=1, device_id=(partner(me, d, n_sp), t), device_id_type=MESH)
    for j in range(1, n_tp):
        pl.semaphore_signal(barrier, inc=1, device_id=(me, lax.rem(t + j, n_tp)), device_id_type=MESH)

    cols_own = pl.ds(pl.multiple_of(t * C, C), C)
    early = [
        pltpu.make_async_copy(ow_hbm, ow, o_sem.at[0]),
        pltpu.make_async_copy(res_hbm.at[:, cols_own], res, o_sem.at[1]),
    ]
    loads = [
        pltpu.make_async_copy(src, dst, w_sem.at[i])
        for i, (src, dst) in enumerate(((wg_hbm, wg), (wu_hbm, wu), (wd_hbm, wd)))
    ]
    for cp in early + loads:
        cp.start()

    def gated(v, g):
        g = g.astype(F32)
        return v.astype(F32) / (1.0 + jnp.exp(-g))

    H = halo_rows
    G[H:H + T, :] = gated(value[...], gate[...])

    pl.semaphore_wait(barrier, n_sp - 1 + n_tp - 1)

    def remote(src, dst, s_sem, r_sem, dev, start=True):
        cp = pltpu.make_async_remote_copy(
            src_ref=src, dst_ref=dst, send_sem=s_sem, recv_sem=r_sem, device_id=dev, device_id_type=MESH
        )
        if start:
            cp.start()
        return cp

    after = lax.rem(me + 1, n_sp)
    tails = [
        remote(x.at[pl.ds(T - H, H)], halo.at[i], h_s.at[i], h_r.at[i], (after, t), start=False)
        for i, x in enumerate((value, gate))
    ]

    @pl.when(me < n_sp - 1)
    def _():
        for cp in tails:
            cp.start()

    row_ids = ids[...].astype(F32)
    experts = lax.broadcasted_iota(jnp.int32, (n_sp, T), 0).astype(F32)
    hot = [jnp.where(experts == row_ids[k:k + 1, :], 1.0, 0.0) for k in range(top)]
    counts = functools.reduce(jnp.add, hot)
    before = lax.broadcasted_iota(jnp.int32, (T, T), 0) < lax.broadcasted_iota(jnp.int32, (T, T), 1)
    earlier = jnp.dot(
        counts.astype(BF16), jnp.where(before, 1.0, 0.0).astype(BF16), preferred_element_type=F32
    )
    target = [
        row_ids[k:k + 1, :] * cap + jnp.sum(hot[k] * earlier, axis=0, keepdims=True) for k in range(top)
    ]
    slots = lax.broadcasted_iota(jnp.int32, (n_sp * cap, T), 0).astype(F32)
    pickt[...] = functools.reduce(
        jnp.add, [jnp.where(slots == target[k], 1.0, 0.0) for k in range(top)]
    ).astype(BF16)
    meta[...] = as_columns(stacked(target + [rwt[k:k + 1, :] for k in range(top)]))

    step_rows, step_lanes = 64, min(128, chans)
    taps32 = taps[...].astype(F32)

    def filter_rows(r):
        for l in range(0, chans, step_lanes):
            total = jnp.zeros((step_rows, step_lanes), F32)
            for i in range(taps_count):
                at = H - taps_count + 1 + r + i
                total = total + taps32[i:i + 1, l:l + step_lanes] * G[at:at + step_rows, l:l + step_lanes]
            fil[r:r + step_rows, l:l + step_lanes] = total

    for r in range(step_rows, T, step_rows):
        filter_rows(r)

    @pl.when(me > 0)
    def _():
        for cp in tails:
            cp.wait_recv()
        G[0:H, :] = gated(halo[0], halo[1])

    @pl.when(me == 0)
    def _():
        G[0:H, :] = jnp.zeros((H, chans), F32)

    filter_rows(0)

    sent = []

    def over_tp(which, rows8):
        st_s[which] = rows8
        cps = []
        for j in range(1, n_tp):
            i = which * n_tp + j
            cps.append(
                remote(st_s.at[which], st_r.at[i], s_s.at[i], s_r.at[i], (me, lax.rem(t + j, n_tp)))
            )
        total = rows8
        for j, cp in enumerate(cps):
            cp.wait_recv()
            total = total + st_r[which * n_tp + j + 1]
        sent.extend(cps)
        return total

    f = fil[...]
    sums = over_tp(0, as_row(jnp.sum(f, axis=1, keepdims=True), jnp.sum(f * f, axis=1, keepdims=True)))
    channels = chans * n_tp
    average = sums[0:1] / channels
    variance = sums[1:2] / channels - average * average
    cols = as_columns(stacked([average, lax.rsqrt(variance + 1e-05)]))
    normed = (fil[...] - cols[:, 0:1]) * cols[:, 1:2] * gain[...]
    act[...] = (normed / (1.0 + jnp.exp(-normed))).astype(BF16)
    for cp in early:
        cp.wait()

    p1 = {}
    for k in list(range(1, Y)) + [0]:
        yy = lax.rem(y + k, Y)
        at = pl.ds(pl.multiple_of((yy * 2 + 1 - c) * C, C), C)
        p1s[k] = jnp.dot(act[...], ow[:, at], preferred_element_type=F32).astype(BF16)
        p1[k] = remote(p1s.at[k], p1r.at[k], p1_s.at[k], p1_r.at[k], (me, core))
    for k in list(range(1, Y)) + [0]:
        yy = lax.rem(y + k, Y)
        at = pl.ds(pl.multiple_of((yy * 2 + c) * C, C), C)
        p1own[k] = jnp.dot(act[...], ow[:, at], preferred_element_type=F32)
    y1 = {}
    for k in range(1, Y):
        p1[k].wait_recv()
        y1s[k] = (p1own[k] + p1r[k].astype(F32)).astype(BF16)
        y1[k] = remote(y1s.at[k], y1r.at[k], y1_s.at[k], y1_r.at[k], (me, ypeer(k)))
    p1[0].wait_recv()
    stream = res[...].astype(F32) + p1own[0] + p1r[0].astype(F32)
    for k in range(1, Y):
        y1[k].wait_recv()
        stream = stream + y1r[k].astype(F32)
    own[...] = stream
    sent.extend(p1.values())
    sent.extend(y1.values())
    square = jnp.sum(stream * stream, axis=1, keepdims=True)
    squares = over_tp(1, as_row(square, jnp.zeros_like(square)))
    scale = as_columns(stacked([lax.rsqrt(squares[0:1] / (C * n_tp) + 1e-06)]))[:, 0:1]
    nrm[...] = (own[...] * scale).astype(BF16)

    arrive = {}
    for p, d in enumerate(order):
        dst = partner(me, d, n_sp)
        at = pl.ds(pl.multiple_of(dst * cap, cap), cap)
        block = jnp.dot(pickt[at, :], nrm[...], preferred_element_type=F32).astype(BF16)
        if d == 0:
            X[t, p * cap:(p + 1) * cap, :] = block
        else:
            mine = pl.ds(p * cap, cap)
            send[mine, :] = block
            cp = remote(send.at[mine], X.at[t, mine], a_s.at[p], a_r.at[p], (dst, t))
            sent.append(cp)
            arrive[p] = cp

    ag_c, ag_y, ag_f, rs_c, rs_y, ret = {}, {}, {}, {}, {}, {}

    def rows(s):
        return pl.ds(s * R, R)

    def stage_a(s):
        for p in range(s * group, (s + 1) * group):
            if order[p] != 0:
                arrive[p].wait_recv()
        mine = X.at[t, rows(s)]
        for k in range(1, Y):
            i = s * Y + k
            ag_y[s, k] = remote(mine, mine, y_s.at[i], y_r.at[i], (me, ypeer(k)))
        ag_c[s] = remote(mine, mine, c_s.at[s], c_r.at[s], (me, core))

    def stage_b(s):
        for k in range(1, Y):
            ag_y[s, k].wait_recv()
            i = s * Y + k
            got = X.at[lax.rem(y + Y - k, Y) * 2 + c, rows(s)]
            ag_f[s, k] = remote(got, got, f_s.at[i], f_r.at[i], (me, core))

    tile = 256

    def stage_c(s):
        ag_c[s].wait_recv()
        for k in range(1, Y):
            ag_f[s, k].wait_recv()
        for j in range(n_tp):
            xs[:, j * C:(j + 1) * C] = X[j, rows(s), :]
        if s == 0:
            for cp in loads:
                cp.wait()

        def up(n, carry):
            cols = pl.ds(pl.multiple_of(n * tile, tile), tile)
            x = xs[...]
            g = jnp.dot(x, wg[:, cols], preferred_element_type=F32)
            u = jnp.dot(x, wu[:, cols], preferred_element_type=F32)
            hid[:, cols] = (g / (1.0 + jnp.exp(-g)) * u).astype(BF16)
            return carry

        lax.fori_loop(0, hid.shape[1] // tile, up, 0)

        def theirs(yy, carry):
            cols = pl.ds(pl.multiple_of((yy * 2 + 1 - c) * C, C), C)
            pcs[s, yy] = jnp.dot(hid[...], wd[:, cols], preferred_element_type=F32).astype(BF16)
            return carry

        lax.fori_loop(0, Y, theirs, 0)
        rs_c[s] = remote(pcs.at[s], pcr.at[s], pc_s.at[s], pc_r.at[s], (me, core))

        def ours(yy, carry):
            cols = pl.ds(pl.multiple_of((yy * 2 + c) * C, C), C)
            pown[yy] = jnp.dot(hid[...], wd[:, cols], preferred_element_type=F32)
            return carry

        lax.fori_loop(0, Y, ours, 0)

    def stage_d(s):
        rs_c[s].wait_recv()
        for k in range(1, Y):
            yy = lax.rem(y + k, Y)
            i = s * Y + k
            pys[i] = (pown[yy] + pcr[s, yy].astype(F32)).astype(BF16)
            rs_y[s, k] = remote(pys.at[i], pyr.at[i], py_s.at[i], py_r.at[i], (me, ypeer(k)))
        q[s] = pown[y] + pcr[s, y].astype(F32)

    def stage_e(s):
        total = q[s]
        for k in range(1, Y):
            rs_y[s, k].wait_recv()
            total = total + pyr[s * Y + k].astype(F32)
        eo[rows(s)] = total.astype(BF16)
        for p in range(s * group, (s + 1) * group):
            d = order[p]
            dst = partner(me, d, n_sp)
            src = eo.at[pl.ds(p * cap, cap)]
            to = back.at[pl.ds(pl.multiple_of(me * cap, cap), cap)]
            if d == 0:
                cp = pltpu.make_async_copy(src, to, l_sem.at[1])
                cp.start()
            else:
                cp = remote(src, to, b_s.at[p], b_r.at[p], (dst, t))
            ret[p] = cp

    stage_a(0)
    stage_b(0)
    for s in range(S):
        if s + 1 < S:
            stage_a(s + 1)
        stage_c(s)
        if s + 1 < S:
            stage_b(s + 1)
        stage_d(s)
        if s > 0:
            stage_e(s - 1)
    stage_e(S - 1)

    for p, d in enumerate(order):
        if d == 0:
            ret[p].wait()
        else:
            ret[p].wait_recv()
    total = own[...]
    places = lax.broadcasted_iota(jnp.int32, (total.shape[0], back.shape[0]), 1).astype(F32)
    for k in range(top):
        pick = jnp.where(places == meta[:, k:k + 1], 1.0, 0.0).astype(BF16)
        total = total + meta[:, top + k:top + k + 1] * jnp.dot(pick, back[...], preferred_element_type=F32)
    out[...] = total.astype(BF16)

    @pl.when(me < n_sp - 1)
    def _():
        for cp in tails:
            cp.wait_send()

    for cp in sent:
        cp.wait_send()
    for table in (ag_c, ag_y, ag_f, rs_c, rs_y):
        for cp in table.values():
            cp.wait_send()
    for p, d in enumerate(order):
        if d != 0:
            ret[p].wait_send()


def local(
    conv_value,
    conv_gate,
    conv_taps,
    conv_gain,
    out_weight,
    residual,
    route_ids,
    route_weight,
    expert_gate,
    expert_up,
    expert_down,
):
    n_sp, n_tp = lax.axis_size("sp"), lax.axis_size("tp")
    T, chans = conv_value.shape
    top = route_ids.shape[1]
    width, hidden = expert_gate.shape[1:]
    cap = 2 * T * top // n_sp
    C = width // n_tp
    halo_rows = -(-(conv_taps.shape[0] - 1) // 16) * 16
    group = max(1, min(n_sp, 256 // cap))
    order = list(range(n_sp))
    if n_sp == 8:
        order = [0, 1, 4, 5, 6, 7, 2, 3]
    S, Y, R = n_sp // group, n_tp // 2, cap * group
    dma = pltpu.SemaphoreType.DMA
    vm = pl.BlockSpec(memory_space=pltpu.VMEM)
    hb = pl.BlockSpec(memory_space=pl.ANY)
    return pl.pallas_call(
        functools.partial(layer_kernel, n_sp, n_tp, cap, order, group, halo_rows),
        out_shape=jax.ShapeDtypeStruct((T, C), BF16),
        in_specs=[vm] * 6 + [hb] * 5,
        out_specs=vm,
        scratch_shapes=[
            pltpu.VMEM((chans, width), BF16),
            pltpu.VMEM((T, C), BF16),
            pltpu.VMEM((2, halo_rows, chans), BF16),
            pltpu.VMEM((halo_rows + T, chans), F32),
            pltpu.VMEM((T, chans), F32),
            pltpu.VMEM((2, 8, T), F32),
            pltpu.VMEM((2 * n_tp, 8, T), F32),
            pltpu.VMEM((T, chans), BF16),
            pltpu.VMEM((Y, T, C), BF16),
            pltpu.VMEM((Y, T, C), BF16),
            pltpu.VMEM((Y, T, C), F32),
            pltpu.VMEM((Y, T, C), BF16),
            pltpu.VMEM((Y, T, C), BF16),
            pltpu.VMEM((T, C), F32),
            pltpu.VMEM((T, C), BF16),
            pltpu.VMEM((n_sp * cap, T), BF16),
            pltpu.VMEM((T, 128), F32),
            pltpu.VMEM((n_sp * cap, C), BF16),
            pltpu.VMEM((width, hidden), BF16),
            pltpu.VMEM((width, hidden), BF16),
            pltpu.VMEM((hidden, width), BF16),
            pltpu.VMEM((n_tp, n_sp * cap, C), BF16),
            pltpu.VMEM((R, width), BF16),
            pltpu.VMEM((R, hidden), BF16),
            pltpu.VMEM((Y, R, C), F32),
            pltpu.VMEM((S, Y, R, C), BF16),
            pltpu.VMEM((S, Y, R, C), BF16),
            pltpu.VMEM((S, R, C), F32),
            pltpu.VMEM((S * Y, R, C), BF16),
            pltpu.VMEM((S * Y, R, C), BF16),
            pltpu.VMEM((n_sp * cap, C), BF16),
            pltpu.VMEM((n_sp * cap, C), BF16),
            dma((2,)), dma((2,)), dma((2,)),
            dma((2 * n_tp,)), dma((2 * n_tp,)),
            dma((Y,)), dma((Y,)),
            dma((Y,)), dma((Y,)),
            dma((3,)), dma((2,)),
            dma((n_sp,)), dma((n_sp,)),
            dma((S,)), dma((S,)),
            dma((S * Y,)), dma((S * Y,)),
            dma((S * Y,)), dma((S * Y,)),
            dma((S,)), dma((S,)),
            dma((S * Y,)), dma((S * Y,)),
            dma((n_sp,)), dma((n_sp,)),
        ],
        compiler_params=pltpu.CompilerParams(
            collective_id=1, has_side_effects=True, vmem_limit_bytes=60 * 1024 * 1024
        ),
    )(
        conv_value, conv_gate, conv_taps, conv_gain.reshape(1, chans), route_ids.T, route_weight.T,
        out_weight, residual, expert_gate[0], expert_up[0], expert_down[0],
    )


def solution(mesh):
    placed = (
        P("sp", "tp"),
        P("sp", "tp"),
        P(None, "tp"),
        P("tp"),
        P("tp", None),
        P("sp", None),
        P("sp", None),
        P("sp", None),
        P("sp", None, "tp"),
        P("sp", None, "tp"),
        P("sp", "tp", None),
    )
    return jax.shard_map(
        local, mesh=mesh, in_specs=placed, out_specs=P("sp", "tp"), check_vma=False
    )
```

time: 147 us -> 102 us (0.69)
  waiting for transfers between devices: 22.9 us -> 0 us
  Pallas kernels: 78.4 us -> 99.8 us
  between operations: 13.6 us -> 0.01 us
  blocking collectives: 12.1 us -> 0 us
  other arithmetic: 6.73 us -> 0 us
  starting transfers between devices: 4.87 us -> 0 us
  local copies, waits for them, and re-layouts: 5.14 us -> 1.67 us
  matrix products: 3.03 us -> 0 us
    reduce_scatter x1 -> x0, waiting for transfers between devices: 22.9 us -> none  [local(): lax.psum_scatter(jnp.dot(activated, out_weight, preferred_element_type=F3...]
    pallas_call x1, Pallas kernels: 78.4 us -> 99.8 us  [local(): pl.pallas_call(functools.partial(layer_kernel, n_sp, n_tp, cap, order, gr...]
    psum x2 -> x0, blocking collectives: 12.1 us -> none  [the longest x1 6.33 us: local(): lax.psum((jnp.sum(filtered, axis=1), jnp.sum(filtered * filtered, axis=1)...]
    ppermute x1 -> x0, starting transfers between devices: 4.87 us -> none  [passed_along(): lax.ppermute(value, axis, [(source, source + steps) for source in range(i...]
    mul x4 -> x0, other arithmetic: 3.07 us -> none  [the longest x2 1.98 us: local(): conv_taps[offset].astype(F32) * gated[offset:offset + token_rows]]
    dot_general x2 -> x0, matrix products: 3.03 us -> none  [the longest x1 1.52 us: local(): send = jnp.dot(pick, normal, preferred_element_type=F32).astype(BF16)]
    reduce_sum x3 -> x0, other arithmetic: 2.43 us -> none  [the longest x1 1.19 us: local(): squares = lax.psum(jnp.sum(own * own, axis=1, keepdims=True), 'tp') / width]
    slice x5 -> x0, local copies, waits for them, and re-layouts: 1.96 us -> none  [the longest x1 0.81 us: local(): conv_value[token_rows - taps_count + 1:]]
  transfers between devices with their start and end apart: 2 -> 0, of which waited for: 1 -> 0; matrix products, arithmetic and copies ran while one was open for 4% -> 0% of each run, Pallas kernels for 0% -> 0%
where the time goes in v2:
time: 102 us; the launch traced here: 101 us
  Pallas kernels  99.8 us (98%)
  local copies, waits for them, and re-layouts  1.67 us (2%)
    pallas_call x1, Pallas kernels, local(): pl.pallas_call(functools.partial(layer_kernel, n_sp, n_tp, cap, order, gr...  99.8 us

profile of v2, /device:TPU:0, one launch (start us, length us, event | category | flops | bytes accessed | tf_op | source)
XLA Modules:
  0.0 101.5 jit_solution(6942361067254904448)
XLA Ops:
  0.0 99.8 %shard_map.109 = bf16[256,512]{1,0:T(8,128)(2,1)} custom-call(bf16[256,256]{1,0:T(8,128)(2,1)} %value.1, bf16[256,256]{1,0:T(8,128)(2,1)} %gate.1, bf16[31,256]{1,0:T(8,128)(2,1)} %taps.1, f32[1,256]{1,0:T(1,128)} %bitcast.11, s32[2,256]{1,0:T(2,128)} %bitcast.9, f32[2,256]{1,0:T(2,128)} %bitcast.10, bf16[256,2048]{1,0:T(8,128)(2,1)} %ow_hbm.1, ...), custom_call_target="tpu_custom_call" | custom-call | tf_op jit(solution)/shard_map/pallas_call | solution.py:381
  99.8 1.7 %copy.13 = bf16[256,512]{1,0:T(8,128)(2,1)} copy(bf16[256,512]{1,0:T(8,128)(2,1)} %shard_map.109) | data formatting | bytes 524288
